TPU v7x, 256 devices: a whole 4x4x8 slice. The times are simulated.
256 devices in a mesh: gr: 2 (over z_hi), fs: 16 (over z_lo, x), tp: 8 (over y, core).
Axes of the slice: x: 4, y: 4, z: 8 (z_hi: 2, z_lo: 4; z = z_hi * 4 + z_lo), core: 2. Of those that a mesh axis runs over, the one named last changes fastest.
Arguments:
- tokens: bfloat16 [32768, 2048], P(('gr', 'fs', 'tp')), may hold values from -6 to 6
- norm_gain: float32 [2048], P('fs'), may hold values from 0.1 to 1.9
- gate_master: float32 [128, 2048, 256], P(None, 'fs', ('gr', 'tp')), may hold values from -0.125 to 0.125
- up_master: float32 [128, 2048, 256], P(None, 'fs', ('gr', 'tp')), may hold values from -0.125 to 0.125
- down_master: float32 [128, 256, 2048], P(None, 'fs', ('gr', 'tp')), may hold values from -0.375 to 0.375
- route_group: int32 [32768], P(('gr', 'fs', 'tp')), may hold values from 0 to 3
- route_expert: int32 [32768, 2], P(('gr', 'fs', 'tp')), may hold values from 0 to 31, all different within a row
- route_weight: float32 [32768, 2], P(('gr', 'fs', 'tp')), may hold values from 0.1 to 1
Outputs:
- gate_new: bfloat16 [128, 2048, 256], P(('fs', 'tp'))
- up_new: bfloat16 [128, 2048, 256], P(('fs', 'tp'))
- down_new: bfloat16 [128, 256, 2048], P(('fs', 'tp'))
- mixed: bfloat16 [32768, 2048], P(('gr', 'fs', 'tp'))
Inputs may be any that keep to these rules, and one draw needn't show every extreme that they name: `route_expert`: the 2 entries of a row are different.
All inputs are finite; a program needn't handle non-finite values.
Results may differ from a plain program's by a relative error of at most 0.0086.
Values may be sent and summed in bfloat16 or wider, within the bound.
A program may use at most 64 MiB of HBM per device.

v0:
```python
import jax
import jax.numpy as jnp
from jax import lax
from jax.sharding import PartitionSpec as P

E_GROUPS = 4
TOP = 2


def cut_along(shard, dim, count):
    before, after = (shard.shape[:dim], shard.shape[dim + 1 :])
    return jnp.moveaxis(shard.reshape(*before, count, -1, *after), dim, 0)


def joined_along(pieces, dim):
    pieces = jnp.moveaxis(pieces, 0, dim)
    dims = pieces.shape
    return pieces.reshape(*dims[:dim], dims[dim] * dims[dim + 1], *dims[dim + 2 :])


def joined_exchange(shard, axis, axes, splits, concats):
    sizes = [lax.axis_size(a) for a in axes]
    pieces = cut_along(shard, splits[0], sizes[0])
    pieces = jnp.moveaxis(cut_along(pieces, splits[1] + 1, sizes[1]), 0, 1)
    inside = pieces.shape[2:]
    pieces = pieces.reshape(-1, *inside)
    pieces = lax.all_to_all(pieces, axis, split_axis=0, concat_axis=0, tiled=True)
    pieces = joined_along(pieces.reshape(*sizes, *inside), concats[0] + 1)
    return joined_along(pieces, concats[1])


def sent_to_all(shard, axis):
    count = lax.axis_size(axis)
    return lax.all_to_all(
        jnp.broadcast_to(shard[None], (count, *shard.shape)), axis, 0, 0, tiled=True
    )


def gathered_copies(shard, axis, dim):
    return joined_along(sent_to_all(shard, axis), dim)


def sent_together(arrays, axis, dim, along):
    ends, at = ([], 0)
    for a in arrays[:-1]:
        at += a.shape[along]
        ends.append(at)
    both = jnp.concatenate(arrays, axis=along)
    return tuple(jnp.split(gathered_copies(both, axis, dim), ends, axis=along))


def body(
    tokens, norm_gain, gate_master, up_master, down_master, route_group, route_expert, route_weight
):
    n_fs = lax.axis_size("fs")
    n_tp = lax.axis_size("tp")
    n_gr = lax.axis_size("gr")
    experts = n_fs * n_tp
    per_group = experts // E_GROUPS
    gate_cast = (gate_master * norm_gain[None, :, None]).astype(jnp.bfloat16)
    up_cast = (up_master * norm_gain[None, :, None]).astype(jnp.bfloat16)
    down_cast = down_master.astype(jnp.bfloat16)

    def to_grid(tile):
        return tile.reshape((n_fs, n_tp, 1, tile.shape[1], tile.shape[2]))

    grids = (
        to_grid(jnp.swapaxes(gate_cast, 1, 2)),
        to_grid(jnp.swapaxes(up_cast, 1, 2)),
        to_grid(down_cast),
    )
    grids = (
        joined_exchange(grids[0], ("fs", "tp"), ("fs", "tp"), (0, 1), (4, 3)),
        joined_exchange(grids[1], ("fs", "tp"), ("fs", "tp"), (0, 1), (4, 3)),
        joined_exchange(grids[2], ("fs", "tp"), ("fs", "tp"), (0, 1), (4, 3)),
    )
    grids = sent_together((grids[0], grids[1], grids[2]), "gr", 2, 0)

    def rows_to_matrix(grid):
        hidden_units = grid.shape[2] * grid.shape[3]
        return jnp.swapaxes(grid.reshape(hidden_units, grid.shape[4]), 0, 1)[None]

    gate_new = rows_to_matrix(grids[0])
    up_new = rows_to_matrix(grids[1])
    grid = grids[2]
    f_local = grid.shape[3] // n_tp
    d_local = grid.shape[4] // n_fs
    parts = grid.reshape(n_gr, n_tp, f_local, n_fs, d_local)
    parts = jnp.transpose(parts, (3, 2, 0, 1, 4))
    down_new = parts.reshape(1, n_fs * f_local, n_gr * n_tp * d_local)
    width = tokens.shape[1]
    count = tokens.shape[0]
    floats = tokens.astype(jnp.float32)
    normed = (floats * lax.rsqrt(jnp.mean(floats * floats, axis=-1, keepdims=True) + 1e-06)).astype(
        jnp.bfloat16
    )
    capacity = 3 * count * TOP // (2 * experts)
    flat_ids = (route_group[:, None] * per_group + route_expert).reshape(-1)
    columns = lax.broadcasted_iota(jnp.int32, (flat_ids.shape[0], experts), 1)
    onehot = (flat_ids[:, None] == columns).astype(jnp.int32)
    rank = jnp.sum((jnp.cumsum(onehot, axis=0) - 1) * onehot, axis=1)
    dump = experts * capacity
    slot = jnp.where(rank < capacity, flat_ids * capacity + rank, dump)
    rows = jnp.repeat(normed, TOP, axis=0)
    outgoing = (
        jnp.zeros((dump + 1, width), jnp.bfloat16)
        .at[slot]
        .set(rows)[:-1]
        .reshape(experts, capacity, width)
    )
    block = lax.all_to_all(outgoing, ("fs", "tp"), split_axis=0, concat_axis=0, tiled=True)
    flat_rows = block.reshape(-1, width)
    gate = jnp.dot(flat_rows, gate_new[0], preferred_element_type=jnp.float32)
    upper = jnp.dot(flat_rows, up_new[0], preferred_element_type=jnp.float32)
    hidden = (jax.nn.silu(gate) * upper).astype(jnp.bfloat16)
    result = jnp.dot(hidden, down_new[0], preferred_element_type=jnp.float32).astype(jnp.bfloat16)
    outcome = result.reshape(block.shape)
    returned = lax.all_to_all(outcome, ("fs", "tp"), split_axis=0, concat_axis=0, tiled=True)
    table = jnp.concatenate(
        [returned.reshape(-1, width), jnp.zeros((1, width), jnp.bfloat16)], axis=0
    )
    picked = table[slot].reshape(count, TOP, width).astype(jnp.float32)
    mixed = jnp.sum(picked * route_weight[:, :, None], axis=1).astype(jnp.bfloat16)
    return (gate_new, up_new, down_new, mixed)


def solution(mesh):
    placed = (
        P(("gr", "fs", "tp"), None),
        P("fs"),
        P(None, "fs", ("gr", "tp")),
        P(None, "fs", ("gr", "tp")),
        P(None, "fs", ("gr", "tp")),
        P(("gr", "fs", "tp")),
        P(("gr", "fs", "tp"), None),
        P(("gr", "fs", "tp"), None),
    )
    return jax.shard_map(
        body,
        mesh=mesh,
        in_specs=placed,
        out_specs=(
            P(("fs", "tp"), None, None),
            P(("fs", "tp"), None, None),
            P(("fs", "tp"), None, None),
            P(("gr", "fs", "tp"), None),
        ),
        check_vma=False,
    )
```

profile of v0, /device:TPU:1, one launch (start us, length us, event | category | flops | bytes accessed | tf_op | source)
XLA Modules:
  0.0 312.1 jit_solution(5620391754165281785)
XLA Ops:
  0.7 2.7 fusion.5
  3.4 14.0 %all-to-all-start.1 = ((bf16[128,1,1,1,16,128]{5,4,3,2,1,0:T(8,128)(2,1)}), bf16[128,1,1,1,16,128]{5,4,3,2,1,0:T(8,128)(2,1)S(1)}, u32[]{:S(2)}, u32[]{:S(2)}) async-start(bf16[128,1,1,1,16,128]{5,4,3,2,1,0:T(8,128)(2,1)} %get-tuple-element.10), calls=%async_computation.1 | async-start | bytes 1048576 | tf_op jit(solution)/shard_map/all_to_all | solution.py:27
  17.9 17.6 %all-to-all-done.1 = bf16[128,1,1,1,16,128]{5,4,3,2,1,0:T(8,128)(2,1)S(1)} async-done(((bf16[128,1,1,1,16,128]{5,4,3,2,1,0:T(8,128)(2,1)}), bf16[128,1,1,1,16,128]{5,4,3,2,1,0:T(8,128)(2,1)S(1)}, u32[]{:S(2)}, u32[]{:S(2)}) %all-to-all-start.1) | async-done | bytes 524320 | tf_op jit(solution)/shard_map/all_to_all | solution.py:27
  35.5 6.4 %all-to-all-start = ((bf16[128,1,1,1,16,128]{5,4,3,2,1,0:T(8,128)(2,1)}), bf16[128,1,1,1,16,128]{5,4,3,2,1,0:T(8,128)(2,1)S(1)}, u32[]{:S(2)}, u32[]{:S(2)}) async-start(bf16[128,1,1,1,16,128]{5,4,3,2,1,0:T(8,128)(2,1)} %get-tuple-element.9), calls=%async_computation | async-start | bytes 1048576 | tf_op jit(solution)/shard_map/all_to_all | solution.py:27
  43.6 16.6 %all-to-all-done = bf16[128,1,1,1,16,128]{5,4,3,2,1,0:T(8,128)(2,1)S(1)} async-done(((bf16[128,1,1,1,16,128]{5,4,3,2,1,0:T(8,128)(2,1)}), bf16[128,1,1,1,16,128]{5,4,3,2,1,0:T(8,128)(2,1)S(1)}, u32[]{:S(2)}, u32[]{:S(2)}) %all-to-all-start) | async-done | bytes 524320 | tf_op jit(solution)/shard_map/all_to_all | solution.py:27
  60.3 7.5 %all-to-all-start.2 = ((bf16[128,1,1,1,16,128]{5,4,3,2,1,0:T(8,128)(2,1)}), bf16[128,1,1,1,16,128]{5,4,3,2,1,0:T(8,128)(2,1)}, u32[]{:S(2)}, u32[]{:S(2)}) async-start(bf16[128,1,1,1,16,128]{5,4,3,2,1,0:T(8,128)(2,1)} %convert_bitcast_fusion), calls=%async_computation.2 | async-start | bytes 1048576 | tf_op jit(solution)/shard_map/all_to_all | solution.py:27
  69.2 2.6 scatter_custom_fusion
  72.0 2.3 reshape.130
  74.3 11.4 %all-to-all-done.2 = bf16[128,1,1,1,16,128]{5,4,3,2,1,0:T(8,128)(2,1)} async-done(((bf16[128,1,1,1,16,128]{5,4,3,2,1,0:T(8,128)(2,1)}), bf16[128,1,1,1,16,128]{5,4,3,2,1,0:T(8,128)(2,1)}, u32[]{:S(2)}, u32[]{:S(2)}) %all-to-all-start.2) | async-done | bytes 524320 | tf_op jit(solution)/shard_map/all_to_all | solution.py:27
  85.7 6.6 %all-to-all-start.4 = ((bf16[128,3,2048]{2,1,0:T(4,128)(2,1)}), bf16[128,3,2048]{2,1,0:T(4,128)(2,1)S(1)}, u32[]{:S(2)}, u32[]{:S(2)}) async-start(bf16[128,3,2048]{2,1,0:T(4,128)(2,1)} %reshape.130), calls=%async_computation.4 | async-start | bytes 4194304 | tf_op jit(solution)/shard_map/all_to_all | solution.py:111
  93.5 2.1 reshape_transpose_reshape.10
  96.9 1.4 copy.55
  99.3 2.6 maximum_bitcast_fusion
  101.9 42.4 %all-to-all-done.4 = bf16[128,3,2048]{2,1,0:T(4,128)(2,1)S(1)} async-done(((bf16[128,3,2048]{2,1,0:T(4,128)(2,1)}), bf16[128,3,2048]{2,1,0:T(4,128)(2,1)S(1)}, u32[]{:S(2)}, u32[]{:S(2)}) %all-to-all-start.4) | async-done | bytes 1572896 | tf_op jit(solution)/shard_map/all_to_all | solution.py:111
  144.4 4.2 %broadcast_in_dim.17 = bf16[2,3,1,1,128,2048]{5,4,3,2,1,0:T(8,128)(2,1)} broadcast(bf16[3,128,2048]{2,1,0:T(8,128)(2,1)} %maximum_bitcast_fusion), dimensions={1,4,5} | broadcast | bytes 4718592 | tf_op jit(solution)/shard_map/broadcast_in_dim | solution.py:35
  148.6 5.5 %all-to-all-start.3 = ((bf16[2,3,1,1,128,2048]{5,4,3,2,1,0:T(8,128)(2,1)}), bf16[2,3,1,1,128,2048]{5,4,3,2,1,0:T(8,128)(2,1)S(1)}, u32[]{:S(2)}, u32[]{:S(2)}) async-start(bf16[2,3,1,1,128,2048]{5,4,3,2,1,0:T(8,128)(2,1)} %broadcast_in_dim.17), calls=%async_computation.3 | async-start | bytes 6291456 | tf_op jit(solution)/shard_map/all_to_all | solution.py:34
  154.0 5.1 %reshape.131 = bf16[384,2048]{1,0:T(8,128)(2,1)} reshape(bf16[128,3,2048]{2,1,0:T(4,128)(2,1)} %copy-done.1) | data formatting | bytes 3145728 | tf_op jit(solution)/shard_map/reshape | solution.py:112
  159.1 57.5 %all-to-all-done.3 = bf16[2,3,1,1,128,2048]{5,4,3,2,1,0:T(8,128)(2,1)S(1)} async-done(((bf16[2,3,1,1,128,2048]{5,4,3,2,1,0:T(8,128)(2,1)}), bf16[2,3,1,1,128,2048]{5,4,3,2,1,0:T(8,128)(2,1)S(1)}, u32[]{:S(2)}, u32[]{:S(2)}) %all-to-all-start.3) | async-done | bytes 3145760 | tf_op jit(solution)/shard_map/all_to_all | solution.py:34
  216.6 1.5 fusion.18
  219.1 1.3 squeeze_reshape.3
  220.4 2.1 fusion.19
  222.5 4.7 %convolution_convert_fusion = bf16[384,2048]{1,0:T(8,128)(2,1)} fusion(bf16[256,2048]{1,0:T(8,128)(2,1)} %squeeze_reshape.3, bf16[384,2048]{1,0:T(8,128)(2,1)} %reshape.131, bf16[256,2048]{1,0:T(8,128)(2,1)S(1)} %bitcast.78, f32[384,256]{1,0:T(8,128)S(1)} %fusion.19), kind=kOutput, calls=%fused_computation.2 | convolution fusion | flops 806682624 | bytes 5636096 | tf_op jit(solution)/shard_map/dot_general | solution.py:116
  227.2 5.1 %reshape.132 = bf16[128,3,2048]{2,1,0:T(4,128)(2,1)} reshape(bf16[384,2048]{1,0:T(8,128)(2,1)} %convolution_convert_fusion) | data formatting | bytes 3145728 | tf_op jit(solution)/shard_map/reshape | solution.py:117
  232.3 17.3 %all-to-all-start.5 = ((bf16[128,3,2048]{2,1,0:T(4,128)(2,1)}), bf16[128,3,2048]{2,1,0:T(4,128)(2,1)}, u32[]{:S(2)}, u32[]{:S(2)}) async-start(bf16[128,3,2048]{2,1,0:T(4,128)(2,1)} %reshape.132), calls=%async_computation.5 | async-start | bytes 4194304 | tf_op jit(solution)/shard_map/all_to_all | solution.py:118
  249.8 1.3 reshape.127
  251.1 1.3 copy.41
  252.4 1.3 copy.42
  253.7 47.6 %all-to-all-done.5 = bf16[128,3,2048]{2,1,0:T(4,128)(2,1)} async-done(((bf16[128,3,2048]{2,1,0:T(4,128)(2,1)}), bf16[128,3,2048]{2,1,0:T(4,128)(2,1)}, u32[]{:S(2)}, u32[]{:S(2)}) %all-to-all-start.5) | async-done | bytes 1572896 | tf_op jit(solution)/shard_map/all_to_all | solution.py:118
  301.3 3.9 %reshape.133 = bf16[384,2048]{1,0:T(8,128)(2,1)S(1)} reshape(bf16[128,3,2048]{2,1,0:T(4,128)(2,1)} %all-to-all-done.5) | data formatting | bytes 3145728 | tf_op jit(solution)/shard_map/reshape | solution.py:120
  305.4 1.4 gather_fusion
  306.8 1.3 reshape.134
  308.1 3.9 %multiply_reduce_fusion = bf16[128,2048]{1,0:T(8,128)(2,1)} fusion(f32[128,2,2048]{2,1,0:T(2,128)S(1)} %reshape.134, f32[128,2]{1,0:T(8,128)S(1)} %copy.50), kind=kLoop, calls=%fused_computation.3 | loop fusion | flops 786432 | bytes 2622464 | tf_op jit(solution)/shard_map/reduce_sum | solution.py:123
  (58 shorter events, 8.5 us)
Async XLA Ops:
  0.6 16.7 %copy-start.12 = (s32[128]{0:T(128)S(1)}, s32[128]{0:T(128)}, u32[]{:S(2)}) copy-start(s32[128]{0:T(128)} %param.13) | copy-start | bytes 1540
  0.6 16.7 %copy-start.11 = (s32[128,2]{0,1:T(2,128)S(1)}, s32[128,2]{0,1:T(2,128)}, u32[]{:S(2)}) copy-start(s32[128,2]{0,1:T(2,128)} %param.14) | copy-start | bytes 3076
  3.3 39.2 %copy-start.3 = (bf16[128,2048]{1,0:T(8,128)(2,1)S(1)}, bf16[128,2048]{1,0:T(8,128)(2,1)}, u32[]{:S(2)}) copy-start(bf16[128,2048]{1,0:T(8,128)(2,1)} %param.8) | copy-start | bytes 1572868
  3.4 32.2 %all-to-all-start.1 = ((bf16[128,1,1,1,16,128]{5,4,3,2,1,0:T(8,128)(2,1)}), bf16[128,1,1,1,16,128]{5,4,3,2,1,0:T(8,128)(2,1)S(1)}, u32[]{:S(2)}, u32[]{:S(2)}) async-start(bf16[128,1,1,1,16,128]{5,4,3,2,1,0:T(8,128)(2,1)} %get-tuple-element.10), calls=%async_computation.1 | async-start | bytes 1048576 | tf_op jit(solution)/shard_map/all_to_all | solution.py:27
  17.3 25.4 %copy-start.9 = (f32[128,16,128]{2,1,0:T(8,128)S(1)}, f32[128,16,128]{2,1,0:T(8,128)}, u32[]{:S(2)}) copy-start(f32[128,16,128]{2,1,0:T(8,128)} %param.12) | copy-start | bytes 3145732
  35.5 8.1 %copy-start.4 = (bf16[128,1,1,1,16,128]{5,4,3,2,1,0:T(8,128)(2,1)}, bf16[128,1,1,1,16,128]{5,4,3,2,1,0:T(8,128)(2,1)S(1)}, u32[]{:S(2)}) copy-start(bf16[128,1,1,1,16,128]{5,4,3,2,1,0:T(8,128)(2,1)S(1)} %all-to-all-done.1) | copy-start | bytes 1572868
  35.5 24.7 %all-to-all-start = ((bf16[128,1,1,1,16,128]{5,4,3,2,1,0:T(8,128)(2,1)}), bf16[128,1,1,1,16,128]{5,4,3,2,1,0:T(8,128)(2,1)S(1)}, u32[]{:S(2)}, u32[]{:S(2)}) async-start(bf16[128,1,1,1,16,128]{5,4,3,2,1,0:T(8,128)(2,1)} %get-tuple-element.9), calls=%async_computation | async-start | bytes 1048576 | tf_op jit(solution)/shard_map/all_to_all | solution.py:27
  60.3 8.3 %copy-start.6 = (bf16[128,1,1,1,16,128]{5,4,3,2,1,0:T(8,128)(2,1)}, bf16[128,1,1,1,16,128]{5,4,3,2,1,0:T(8,128)(2,1)S(1)}, u32[]{:S(2)}) copy-start(bf16[128,1,1,1,16,128]{5,4,3,2,1,0:T(8,128)(2,1)S(1)} %all-to-all-done) | copy-start | bytes 1572868
  60.3 25.4 %all-to-all-start.2 = ((bf16[128,1,1,1,16,128]{5,4,3,2,1,0:T(8,128)(2,1)}), bf16[128,1,1,1,16,128]{5,4,3,2,1,0:T(8,128)(2,1)}, u32[]{:S(2)}, u32[]{:S(2)}) async-start(bf16[128,1,1,1,16,128]{5,4,3,2,1,0:T(8,128)(2,1)} %convert_bitcast_fusion), calls=%async_computation.2 | async-start | bytes 1048576 | tf_op jit(solution)/shard_map/all_to_all | solution.py:27
  74.3 18.0 %copy-start.5 = (bf16[128,1,1,1,16,128]{5,4,3,2,1,0:T(8,128)(2,1)S(1)}, bf16[128,1,1,1,16,128]{5,4,3,2,1,0:T(8,128)(2,1)}, u32[]{:S(2)}) copy-start(bf16[128,1,1,1,16,128]{5,4,3,2,1,0:T(8,128)(2,1)} %copy-done.4) | copy-start | bytes 1572868
  85.7 58.7 %all-to-all-start.4 = ((bf16[128,3,2048]{2,1,0:T(4,128)(2,1)}), bf16[128,3,2048]{2,1,0:T(4,128)(2,1)S(1)}, u32[]{:S(2)}, u32[]{:S(2)}) async-start(bf16[128,3,2048]{2,1,0:T(4,128)(2,1)} %reshape.130), calls=%async_computation.4 | async-start | bytes 4194304 | tf_op jit(solution)/shard_map/all_to_all | solution.py:111
  92.3 3.2 %copy-start.7 = (bf16[128,1,1,1,16,128]{5,4,3,2,1,0:T(8,128)(2,1)S(1)}, bf16[128,1,1,1,16,128]{5,4,3,2,1,0:T(8,128)(2,1)}, u32[]{:S(2)}) copy-start(bf16[128,1,1,1,16,128]{5,4,3,2,1,0:T(8,128)(2,1)} %copy-done.6) | copy-start | bytes 1572868
  95.9 3.4 %copy-start.8 = (bf16[1,1,1,128,2048]{4,3,2,1,0:T(8,128)(2,1)S(1)}, bf16[1,1,1,128,2048]{4,3,2,1,0:T(8,128)(2,1)}, u32[]{:S(2)}) copy-start(bf16[1,1,1,128,2048]{4,3,2,1,0:T(8,128)(2,1)} %reshape_transpose_reshape.10) | copy-start | bytes 1572868
  144.4 4.2 %copy-start.1 = (bf16[128,3,2048]{2,1,0:T(4,128)(2,1)}, bf16[128,3,2048]{2,1,0:T(4,128)(2,1)S(1)}, u32[]{:S(2)}) copy-start(bf16[128,3,2048]{2,1,0:T(4,128)(2,1)S(1)} %all-to-all-done.4) | copy-start | bytes 4718596
  148.6 68.1 %all-to-all-start.3 = ((bf16[2,3,1,1,128,2048]{5,4,3,2,1,0:T(8,128)(2,1)}), bf16[2,3,1,1,128,2048]{5,4,3,2,1,0:T(8,128)(2,1)S(1)}, u32[]{:S(2)}, u32[]{:S(2)}) async-start(bf16[2,3,1,1,128,2048]{5,4,3,2,1,0:T(8,128)(2,1)} %broadcast_in_dim.17), calls=%async_computation.3 | async-start | bytes 6291456 | tf_op jit(solution)/shard_map/all_to_all | solution.py:34
  218.4 2.0 copy-start
  220.4 2.1 copy-start.2
  232.3 17.3 %copy-start.10 = (f32[128,2]{0,1:T(2,128)S(1)}, f32[128,2]{0,1:T(2,128)}, u32[]{:S(2)}) copy-start(f32[128,2]{0,1:T(2,128)} %param.15) | copy-start | bytes 3076
  232.3 69.0 %all-to-all-start.5 = ((bf16[128,3,2048]{2,1,0:T(4,128)(2,1)}), bf16[128,3,2048]{2,1,0:T(4,128)(2,1)}, u32[]{:S(2)}, u32[]{:S(2)}) async-start(bf16[128,3,2048]{2,1,0:T(4,128)(2,1)} %reshape.132), calls=%async_computation.5 | async-start | bytes 4194304 | tf_op jit(solution)/shard_map/all_to_all | solution.py:118
where the time goes:
time: 313 us; the launch traced here: 312 us
  waiting for transfers between devices  193 us (62%)
  starting transfers between devices  57.3 us (18%)
  local copies, waits for them, and re-layouts  42.9 us (14%)
  other arithmetic  10.9 us (3%)
  matrix products  6.79 us (2%)
    all_to_all x1, waiting for transfers between devices, sent_to_all(): lax.all_to_all(jnp.broadcast_to(shard[None], (count, *shard.shape)), axis...  57.5 us
    all_to_all x1, waiting for transfers between devices, body(): lax.all_to_all(outcome, ('fs', 'tp'), split_axis=0, concat_axis=0, tiled=...  47.6 us
    all_to_all x3, waiting for transfers between devices, joined_exchange(): lax.all_to_all(pieces, axis, split_axis=0, concat_axis=0, tiled=True)  45.6 us
    all_to_all x1, waiting for transfers between devices, body(): lax.all_to_all(outgoing, ('fs', 'tp'), split_axis=0, concat_axis=0, tiled...  42.4 us
    all_to_all x3, starting transfers between devices, joined_exchange(): lax.all_to_all(pieces, axis, split_axis=0, concat_axis=0, tiled=True)  27.9 us
    all_to_all x1, starting transfers between devices, body(): lax.all_to_all(outcome, ('fs', 'tp'), split_axis=0, concat_axis=0, tiled=...  17.3 us
    all_to_all x1, starting transfers between devices, body(): lax.all_to_all(outgoing, ('fs', 'tp'), split_axis=0, concat_axis=0, tiled...  6.64 us
  transfers between devices with their start and end apart: 6, of which 6 were waited for; matrix products, arithmetic and copies ran while one was open for 9% of the time, Pallas kernels for 0%

commit v1 on v0

v1 whole, which is shorter than its diff:
```python
import functools

import jax
import jax.numpy as jnp
from jax import lax
from jax.experimental import pallas as pl
from jax.experimental.pallas import tpu as pltpu
from jax.sharding import PartitionSpec as P

MESH = pl.DeviceIdType.MESH
BF16 = jnp.bfloat16
F32 = jnp.float32

PLANES, GROUPS, INPLANE = 8, 4, 32
TOK, D, F, CAP = 128, 2048, 256, 3
GROUP_ROWS = INPLANE * CAP
SLOTS = GROUPS * GROUP_ROWS
PAIR_ROWS = 16
EXP_ROWS = INPLANE * PAIR_ROWS
NCH = 4
COLS = D // NCH
FAR_FIRST = (4, 3, 5, 2, 6, 1, 7)


def nt_dot(a, b):
    return lax.dot_general(a, b, (((1,), (1,)), ((), ())), preferred_element_type=F32)


def mm(a, b):
    return jnp.dot(a, b, preferred_element_type=F32)


def kernel(
    gate_in, up_in, down_in, gain, tok_in, group, expert, weight,
    gate_out, up_out, down_out, mixed_out,
    fbuf, wgu, wd, zgu, zd, fgu, fd,
    tokv, xzs, xz, xp, xe, hid,
    gt, ut, dn, go, uo, r, rr, q, t, mix,
    in_sem, out_sem, send_z, send_p, rz_gu, rz_d, rz_t, rz_r, rp_gu, rp_d, rp_t, rp_r,
):
    gr, fs, tp = lax.axis_index("gr"), lax.axis_index("fs"), lax.axis_index("tp")
    zl, x = lax.div(fs, 4), lax.rem(fs, 4)
    y, c = lax.div(tp, 2), lax.rem(tp, 2)
    z = gr * 4 + zl
    me = x * 8 + tp

    def z_device(target):
        return (lax.div(target, 4), lax.rem(target, 4) * 4 + x, tp)

    def hop(j):
        o = lax.rem(j * 11, INPLANE)
        tx = lax.rem(x + lax.div(o, 8), 4)
        ty = lax.rem(y + lax.rem(lax.div(o, 2), 4), 4)
        ttp = ty * 2 + lax.rem(c + lax.rem(o, 2), 2)
        return tx * 8 + ttp, (gr, zl * 4 + tx, ttp)

    def remote(src, dst, send, recv, device):
        pltpu.make_async_remote_copy(
            src_ref=src, dst_ref=dst, send_sem=send, recv_sem=recv, device_id=device, device_id_type=MESH
        ).start()

    def wait_bytes(ref, sem):
        pltpu.make_async_copy(ref, ref, sem).wait()

    barrier = pltpu.get_barrier_semaphore()
    for d in FAR_FIRST:
        pl.semaphore_signal(barrier, inc=1, device_id=z_device(lax.rem(z + d, PLANES)), device_id_type=MESH)

    @pl.loop(1, INPLANE)
    def _(j):
        pl.semaphore_signal(barrier, inc=1, device_id=hop(j)[1], device_id_type=MESH)

    inputs = [
        pltpu.make_async_copy(src, dst, in_sem.at[i])
        for i, (src, dst) in enumerate(
            ((gate_in, fbuf.at[0]), (up_in, fbuf.at[1]), (down_in, fbuf.at[2]), (tok_in, tokv))
        )
    ]
    for copy in inputs:
        copy.start()
    inputs[0].wait()
    inputs[1].wait()
    scale = gain[...].reshape(1, 1, 128)

    @pl.loop(0, 16)
    def _(i):
        e = pl.ds(i * 8, 8)
        wgu[e, 0:16, :] = (fbuf[0, e] * scale).astype(BF16)
        wgu[e, 16:32, :] = (fbuf[1, e] * scale).astype(BF16)

    inputs[2].wait()

    @pl.loop(0, 16)
    def _(i):
        e = pl.ds(i * 8, 8)
        wd[e] = fbuf[2, e].astype(BF16)

    pl.semaphore_wait(barrier, len(FAR_FIRST) + INPLANE - 1)

    def send_planes(src, dst, recv):
        for d in FAR_FIRST:
            target = lax.rem(z + d, PLANES)
            experts = pl.ds(lax.rem(target, 4) * INPLANE, INPLANE)
            remote(src.at[experts], dst.at[z], send_z, recv.at[z], z_device(target))

    def forward(src, base, dst, plane, recv):
        @pl.loop(1, INPLANE)
        def _(j):
            place, device = hop(j)
            remote(src.at[base + place], dst.at[plane, me], send_p, recv, device)

    send_planes(wgu, zgu, rz_gu)
    forward(wgu, zl * INPLANE, fgu, z, rp_gu)
    fgu[z, me] = wgu[zl * INPLANE + me]
    fd[z, me] = wd[zl * INPLANE + me]

    inputs[3].wait()

    @pl.loop(0, 4)
    def _(i):
        rows = pl.ds(i * 32, 32)
        v = tokv[rows, :].astype(F32)
        v = v * lax.rsqrt(jnp.mean(v * v, axis=-1, keepdims=True) + 1e-06)
        tokv[rows, :] = v.astype(BF16)

    ids = group[...] * INPLANE + expert[...]
    expert_iota = lax.broadcasted_iota(jnp.int32, (128, TOK), 0)
    one = [(expert_iota == ids[k : k + 1, :]).astype(F32) for k in range(2)]
    lane_iota = lax.broadcasted_iota(jnp.int32, (128, TOK), 1)
    earlier = (expert_iota < lane_iota).astype(BF16)
    count = mm((one[0] + one[1]).astype(BF16), earlier)
    slot_iota = lax.broadcasted_iota(jnp.int32, (SLOTS, TOK), 0)
    pick = []
    for k in range(2):
        rank = jnp.sum(one[k] * count, axis=0, keepdims=True).astype(jnp.int32)
        slot = jnp.where(rank < CAP, ids[k : k + 1, :] * CAP + rank, -1)
        pick.append((slot_iota == slot).astype(F32))
    rows_of = (pick[0] + pick[1]).astype(BF16)
    for n in range(NCH):
        cols = slice(n * COLS, (n + 1) * COLS)
        xzs[:, :, cols] = mm(rows_of, tokv[:, cols]).astype(BF16).reshape(GROUPS, GROUP_ROWS, COLS)
    for d in (3, 2, 1):
        for target, there in ((zl + d, zl + d < GROUPS), (zl - d, zl - d >= 0)):

            @pl.when(there)
            def _(target=target):
                remote(xzs.at[target], xz.at[zl], send_z, rz_t, (gr, target * 4 + x, tp))

    send_planes(wd, zd, rz_d)
    forward(wd, zl * INPLANE, fd, z, rp_d)

    @pl.loop(0, GROUP_ROWS // 16)
    def _(i):
        rows = pl.ds(i * 16, 16)
        xz[zl, rows, :] = xzs[zl, rows, :]

    def relay(d, src, dst, rz, rp):
        plane = lax.rem(z + PLANES - d, PLANES)
        wait_bytes(src.at[plane], rz.at[plane])

        @pl.loop(1, INPLANE)
        def _(j):
            place, device = hop(j)
            remote(src.at[plane, place], dst.at[plane, me], send_p, rp, device)

        dst[plane, me] = src[plane, me]

    for d in FAR_FIRST:
        relay(d, zgu, fgu, rz_gu, rp_gu)

    def placed(i):
        within = i % PAIR_ROWS
        plane = (within >= 3).astype(jnp.int32) + (within >= 6).astype(jnp.int32) + (within >= 9).astype(jnp.int32)
        at = plane * GROUP_ROWS + (i // PAIR_ROWS) * CAP + within - plane * CAP
        return jnp.where(within < GROUPS * CAP, at, -1)

    wait_bytes(xz.at[pl.ds(0, GROUPS - 1)], rz_t)
    order = (
        placed(lax.broadcasted_iota(jnp.int32, (EXP_ROWS, SLOTS), 0))
        == lax.broadcasted_iota(jnp.int32, (EXP_ROWS, SLOTS), 1)
    ).astype(F32).astype(BF16)
    for n in range(NCH):
        cols = slice(n * COLS, (n + 1) * COLS)
        moved = mm(order, xz[:, :, cols].reshape(SLOTS, COLS))
        xp[:, :, cols] = moved.astype(BF16).reshape(INPLANE, PAIR_ROWS, COLS)

    @pl.loop(1, INPLANE)
    def _(j):
        place, device = hop(j)
        remote(xp.at[place], xe.at[me], send_p, rp_t, device)

    xe[me] = xp[me]

    for d in FAR_FIRST[:4]:
        relay(d, zd, fd, rz_d, rp_d)

    wait_bytes(fgu.at[:, pl.ds(0, INPLANE - 1)], rp_gu)
    for h in range(2):
        for s in range(4):
            for px in range(4):
                rows, cols = slice(h * 128, (h + 1) * 128), slice((s * 4 + px) * 128, (s * 4 + px + 1) * 128)
                tiles = slice(px * 8, (px + 1) * 8)
                gt[rows, cols] = fgu[h * 4 + s, tiles, 0:16, :].reshape(128, 128)
                ut[rows, cols] = fgu[h * 4 + s, tiles, 16:32, :].reshape(128, 128)
    wait_bytes(xe.at[pl.ds(0, INPLANE - 1)], rp_t)

    @pl.loop(0, EXP_ROWS // 128)
    def _(i):
        rows = xe[pl.ds(i * 8, 8)].reshape(128, D)
        gate = nt_dot(rows, gt[...])
        upper = nt_dot(rows, ut[...])
        hid[pl.ds(i * 128, 128), :] = (gate / (1.0 + jnp.exp(-gate)) * upper).astype(BF16)

    for d in FAR_FIRST[4:]:
        relay(d, zd, fd, rz_d, rp_d)

    wait_bytes(fd.at[:, pl.ds(0, INPLANE - 1)], rp_d)
    for h in range(2):
        for s in range(4):
            for px in range(4):
                for place in range(8):
                    col = h * 8 + place
                    dn[(s * 4 + px) * 16 : (s * 4 + px + 1) * 16, col * 128 : (col + 1) * 128] = fd[
                        h * 4 + s, px * 8 + place
                    ]
    for n in range(NCH):
        cols = slice(n * COLS, (n + 1) * COLS)
        result = mm(hid[...], dn[:, cols])
        r[n] = result.astype(BF16).reshape(INPLANE, PAIR_ROWS, COLS)

        @pl.loop(1, INPLANE)
        def _(j):
            place, device = hop(j)
            remote(r.at[n, place], rr.at[n, me], send_p, rp_r.at[n], device)

        rr[n, me] = r[n, me]

    back = (
        placed(lax.broadcasted_iota(jnp.int32, (SLOTS, EXP_ROWS), 1))
        == lax.broadcasted_iota(jnp.int32, (SLOTS, EXP_ROWS), 0)
    ).astype(F32).astype(BF16)
    for n in range(NCH):
        wait_bytes(rr.at[n, pl.ds(0, INPLANE - 1)], rp_r.at[n])
        moved = mm(back, rr[n].reshape(EXP_ROWS, COLS))
        q[n] = moved.astype(BF16).reshape(GROUPS, GROUP_ROWS, COLS)
        for d in (3, 2, 1):
            for target, there in ((zl + d, zl + d < GROUPS), (zl - d, zl - d >= 0)):

                @pl.when(there)
                def _(target=target):
                    remote(q.at[n, target], t.at[n, zl], send_z, rz_r.at[n], (gr, target * 4 + x, tp))

        t[n, zl] = q[n, zl]

    down_copy = pltpu.make_async_copy(dn, down_out.at[0], out_sem.at[2])
    down_copy.start()
    for h in range(2):
        for s in range(16):
            rows, cols = slice(h * 128, (h + 1) * 128), slice(s * 128, (s + 1) * 128)
            go[cols, rows] = gt[rows, cols].T
            uo[cols, rows] = ut[rows, cols].T
    gate_copy = pltpu.make_async_copy(go, gate_out.at[0], out_sem.at[0])
    up_copy = pltpu.make_async_copy(uo, up_out.at[0], out_sem.at[1])
    gate_copy.start()
    up_copy.start()

    select = [p.T.astype(BF16) for p in pick]
    weights = [jnp.broadcast_to(weight[k : k + 1, :], (128, TOK)).T[:, 0:1] for k in range(2)]
    for n in range(NCH):
        cols = slice(n * COLS, (n + 1) * COLS)
        wait_bytes(t.at[n, pl.ds(0, GROUPS - 1)], rz_r.at[n])
        table = t[n].reshape(SLOTS, COLS)
        mix[:, cols] = (mm(select[0], table) * weights[0] + mm(select[1], table) * weights[1]).astype(BF16)
    mixed_copy = pltpu.make_async_copy(mix, mixed_out, out_sem.at[3])
    mixed_copy.start()

    others = pl.ds(0, PLANES - 1)
    wait_bytes(zgu.at[others], send_z)
    wait_bytes(zd.at[others], send_z)
    wait_bytes(xz.at[pl.ds(0, GROUPS - 1)], send_z)
    wait_bytes(fgu.at[:, pl.ds(0, INPLANE - 1)], send_p)
    wait_bytes(fd.at[:, pl.ds(0, INPLANE - 1)], send_p)
    wait_bytes(xe.at[pl.ds(0, INPLANE - 1)], send_p)
    for n in range(NCH):
        wait_bytes(t.at[n, pl.ds(0, GROUPS - 1)], send_z)
        wait_bytes(rr.at[n, pl.ds(0, INPLANE - 1)], send_p)
    down_copy.wait()
    gate_copy.wait()
    up_copy.wait()
    mixed_copy.wait()


def body(
    tokens, norm_gain, gate_master, up_master, down_master, route_group, route_expert, route_weight
):
    vmem, hbm = pl.BlockSpec(memory_space=pltpu.VMEM), pl.BlockSpec(memory_space=pl.ANY)
    dma = pltpu.SemaphoreType.DMA
    tile = pltpu.VMEM
    return pl.pallas_call(
        kernel,
        out_shape=(
            jax.ShapeDtypeStruct((1, D, F), BF16),
            jax.ShapeDtypeStruct((1, D, F), BF16),
            jax.ShapeDtypeStruct((1, F, D), BF16),
            jax.ShapeDtypeStruct((TOK, D), BF16),
        ),
        in_specs=[hbm, hbm, hbm, vmem, hbm, vmem, vmem, vmem],
        out_specs=(hbm, hbm, hbm, hbm),
        scratch_shapes=[
            tile((3, 128, 16, 128), F32),
            tile((128, 32, 128), BF16),
            tile((128, 16, 128), BF16),
            tile((PLANES, INPLANE, 32, 128), BF16),
            tile((PLANES, INPLANE, 16, 128), BF16),
            tile((PLANES, INPLANE, 32, 128), BF16),
            tile((PLANES, INPLANE, 16, 128), BF16),
            tile((TOK, D), BF16),
            tile((GROUPS, GROUP_ROWS, D), BF16),
            tile((GROUPS, GROUP_ROWS, D), BF16),
            tile((INPLANE, PAIR_ROWS, D), BF16),
            tile((INPLANE, PAIR_ROWS, D), BF16),
            tile((EXP_ROWS, F), BF16),
            tile((F, D), BF16),
            tile((F, D), BF16),
            tile((F, D), BF16),
            tile((D, F), BF16),
            tile((D, F), BF16),
            tile((NCH, INPLANE, PAIR_ROWS, COLS), BF16),
            tile((NCH, INPLANE, PAIR_ROWS, COLS), BF16),
            tile((NCH, GROUPS, GROUP_ROWS, COLS), BF16),
            tile((NCH, GROUPS, GROUP_ROWS, COLS), BF16),
            tile((TOK, D), BF16),
            dma((4,)),
            dma((4,)),
            dma,
            dma,
            dma((PLANES,)),
            dma((PLANES,)),
            dma,
            dma((NCH,)),
            dma,
            dma,
            dma,
            dma((NCH,)),
        ],
        compiler_params=pltpu.CompilerParams(
            collective_id=0, has_side_effects=True, vmem_limit_bytes=60 * 2**20
        ),
    )(
        jnp.swapaxes(gate_master, 1, 2),
        jnp.swapaxes(up_master, 1, 2),
        down_master,
        norm_gain[None],
        tokens,
        route_group[None],
        route_expert.T,
        route_weight.T,
    )


def solution(mesh):
    placed = (
        P(("gr", "fs", "tp"), None),
        P("fs"),
        P(None, "fs", ("gr", "tp")),
        P(None, "fs", ("gr", "tp")),
        P(None, "fs", ("gr", "tp")),
        P(("gr", "fs", "tp")),
        P(("gr", "fs", "tp"), None),
        P(("gr", "fs", "tp"), None),
    )
    return jax.shard_map(
        body,
        mesh=mesh,
        in_specs=placed,
        out_specs=(
            P(("fs", "tp"), None, None),
            P(("fs", "tp"), None, None),
            P(("fs", "tp"), None, None),
            P(("gr", "fs", "tp"), None),
        ),
        check_vma=False,
    )
```

time: 313 us -> 188 us (0.60)
  waiting for transfers between devices: 193 us -> 0 us
  Pallas kernels: 0 us -> 181 us
  starting transfers between devices: 57.3 us -> 0 us
  local copies, waits for them, and re-layouts: 42.9 us -> 6.15 us
  other arithmetic: 10.9 us -> 0 us
  matrix products: 6.79 us -> 0 us
    all_to_all x6 -> x0, waiting for transfers between devices: 193 us -> none  [the longest x1 57.5 us: sent_to_all(): lax.all_to_all(jnp.broadcast_to(shard[None], (count, *shard.shape)), axis...]
    pallas_call x0 -> x1, Pallas kernels: none -> 181 us  [body(): pl.pallas_call(kernel, out_shape=(jax.ShapeDtypeStruct((1, D, F), BF16),...]
    all_to_all x6 -> x0, starting transfers between devices: 57.3 us -> none  [the longest x3 27.9 us: joined_exchange(): lax.all_to_all(pieces, axis, split_axis=0, concat_axis=0, tiled=True)]
    reshape x11 -> x0, local copies, waits for them, and re-layouts: 23.6 us -> none  [the longest x1 5.14 us: body(): outcome = result.reshape(block.shape)]
    dot_general x2 -> x0, matrix products: 6.79 us -> none  [the longest x1 4.7 us: body(): jnp.dot(hidden, down_new[0], preferred_element_type=jnp.float32)]
    unnamed x28 -> x10, local copies, waits for them, and re-layouts: 0.4 us -> 6.15 us
    another operation x6 -> x0, local copies, waits for them, and re-layouts: 5.37 us -> none  [the longest x3 4.09 us: joined_along(): pieces.reshape(*dims[:dim], dims[dim] * dims[dim + 1], *dims[dim + 2:])]
    broadcast_in_dim x2 -> x0, local copies, waits for them, and re-layouts: 4.83 us -> none  [the longest x1 4.2 us: sent_to_all(): jnp.broadcast_to(shard[None], (count, *shard.shape))]
  transfers between devices with their start and end apart: 6 -> 0, of which waited for: 6 -> 0; matrix products, arithmetic and copies ran while one was open for 9% -> 0% of each run, Pallas kernels for 0% -> 0%
where the time goes in v1:
time: 188 us
  Pallas kernels  181 us (96%)
  local copies, waits for them, and re-layouts  6.15 us (3%)
    pallas_call x1, Pallas kernels, body(): pl.pallas_call(kernel, out_shape=(jax.ShapeDtypeStruct((1, D, F), BF16),...  181 us
    unnamed x10, local copies, waits for them, and re-layouts  6.15 us

profile of v1, /device:TPU:1, one launch (start us, length us, event | category | flops | bytes accessed | tf_op | source)
XLA Modules:
  0.0 187.8 jit_solution(3002579955828420042)
XLA Ops:
  0.6 181.0 %shard_map.111 = (bf16[1,2048,256]{2,1,0:T(8,128)(2,1)}, bf16[1,2048,256]{2,1,0:T(8,128)(2,1)}, bf16[1,256,2048]{2,1,0:T(8,128)(2,1)}, bf16[128,2048]{1,0:T(8,128)(2,1)}) custom-call(f32[128,16,128]{2,1,0:T(8,128)} %bitcast.6, f32[128,16,128]{2,1,0:T(8,128)} %bitcast.7, f32[128,16,128]{2,1,0:T(8,128)} %down_in.1, f32[1,128]{1,0:T(1,128)} %bitcast.10, ...), custom_call_target="tpu_custom_call" | custom-call | tf_op jit(solution)/shard_map/pallas_call | solution.py:299
  181.7 0.0 copy-start.1
  181.7 2.4 %copy.16 = bf16[1,2048,256]{2,1,0:T(8,128)(2,1)} copy(bf16[1,2048,256]{2,1,0:T(8,128)(2,1)} %get-tuple-element.8) | data formatting | bytes 2097152
  184.0 0.0 copy-done.1
  184.0 0.0 copy-start
  184.0 1.0 copy.17
  185.0 0.6 copy-done
  185.6 0.0 copy-start.2
  185.7 1.0 copy.18
  186.6 0.4 copy-done.2
  187.0 0.8 copy.19
Async XLA Ops:
  181.7 2.4 %copy-start.1 = (bf16[1,2048,256]{2,1,0:T(8,128)(2,1)S(1)}, bf16[1,2048,256]{2,1,0:T(8,128)(2,1)}, u32[]{:S(2)}) copy-start(bf16[1,2048,256]{2,1,0:T(8,128)(2,1)} %get-tuple-element.9) | copy-start | bytes 3145732
  184.0 1.6 copy-start
  185.6 1.4 copy-start.2

commit v2 on v1

--- a/solution.py
+++ b/solution.py
@@ -44,6 +44,9 @@
     z = gr * 4 + zl
     me = x * 8 + tp
 
+    row_planes = [z] + [lax.rem(z + step, PLANES) for step in (1, 7, 2 + 4 * c)]
+    row_sources = [z] + [lax.rem(z + step, PLANES) for step in (7, 1, 6 - 4 * c)]
+
     def z_device(target):
         return (lax.div(target, 4), lax.rem(target, 4) * 4 + x, tp)
 
@@ -78,42 +81,6 @@
     ]
     for copy in inputs:
         copy.start()
-    inputs[0].wait()
-    inputs[1].wait()
-    scale = gain[...].reshape(1, 1, 128)
-
-    @pl.loop(0, 16)
-    def _(i):
-        e = pl.ds(i * 8, 8)
-        wgu[e, 0:16, :] = (fbuf[0, e] * scale).astype(BF16)
-        wgu[e, 16:32, :] = (fbuf[1, e] * scale).astype(BF16)
-
-    inputs[2].wait()
-
-    @pl.loop(0, 16)
-    def _(i):
-        e = pl.ds(i * 8, 8)
-        wd[e] = fbuf[2, e].astype(BF16)
-
-    pl.semaphore_wait(barrier, len(FAR_FIRST) + INPLANE - 1)
-
-    def send_planes(src, dst, recv):
-        for d in FAR_FIRST:
-            target = lax.rem(z + d, PLANES)
-            experts = pl.ds(lax.rem(target, 4) * INPLANE, INPLANE)
-            remote(src.at[experts], dst.at[z], send_z, recv.at[z], z_device(target))
-
-    def forward(src, base, dst, plane, recv):
-        @pl.loop(1, INPLANE)
-        def _(j):
-            place, device = hop(j)
-            remote(src.at[base + place], dst.at[plane, me], send_p, recv, device)
-
-    send_planes(wgu, zgu, rz_gu)
-    forward(wgu, zl * INPLANE, fgu, z, rp_gu)
-    fgu[z, me] = wgu[zl * INPLANE + me]
-    fd[z, me] = wd[zl * INPLANE + me]
-
     inputs[3].wait()
 
     @pl.loop(0, 4)
@@ -130,29 +97,62 @@
     earlier = (expert_iota < lane_iota).astype(BF16)
     count = mm((one[0] + one[1]).astype(BF16), earlier)
     slot_iota = lax.broadcasted_iota(jnp.int32, (SLOTS, TOK), 0)
+    away = lax.rem(group[...] - zl + GROUPS, GROUPS)
+    block = jnp.where(away == 2, 3, jnp.where(away == 3, 2, away))
     pick = []
     for k in range(2):
         rank = jnp.sum(one[k] * count, axis=0, keepdims=True).astype(jnp.int32)
-        slot = jnp.where(rank < CAP, ids[k : k + 1, :] * CAP + rank, -1)
+        slot = jnp.where(rank < CAP, block * GROUP_ROWS + expert[k : k + 1, :] * CAP + rank, -1)
         pick.append((slot_iota == slot).astype(F32))
     rows_of = (pick[0] + pick[1]).astype(BF16)
     for n in range(NCH):
         cols = slice(n * COLS, (n + 1) * COLS)
         xzs[:, :, cols] = mm(rows_of, tokv[:, cols]).astype(BF16).reshape(GROUPS, GROUP_ROWS, COLS)
-    for d in (3, 2, 1):
-        for target, there in ((zl + d, zl + d < GROUPS), (zl - d, zl - d >= 0)):
-
-            @pl.when(there)
-            def _(target=target):
-                remote(xzs.at[target], xz.at[zl], send_z, rz_t, (gr, target * 4 + x, tp))
-
-    send_planes(wd, zd, rz_d)
+    inputs[0].wait()
+    inputs[1].wait()
+    scale = gain[...].reshape(1, 1, 128)
+
+    @pl.loop(0, 16)
+    def _(i):
+        e = pl.ds(i * 8, 8)
+        wgu[e, 0:16, :] = (fbuf[0, e] * scale).astype(BF16)
+        wgu[e, 16:32, :] = (fbuf[1, e] * scale).astype(BF16)
+
+    inputs[2].wait()
+
+    @pl.loop(0, 16)
+    def _(i):
+        e = pl.ds(i * 8, 8)
+        wd[e] = fbuf[2, e].astype(BF16)
+
+    pl.semaphore_wait(barrier, len(FAR_FIRST) + INPLANE - 1)
+
+    def send_planes(src, dst, recv, steps):
+        for d in steps:
+            target = lax.rem(z + d, PLANES)
+            experts = pl.ds(lax.rem(target, 4) * INPLANE, INPLANE)
+            remote(src.at[experts], dst.at[z], send_z, recv.at[z], z_device(target))
+
+    def forward(src, base, dst, plane, recv):
+        @pl.loop(1, INPLANE)
+        def _(j):
+            place, device = hop(j)
+            remote(src.at[base + place], dst.at[plane, me], send_p, recv, device)
+
+    for block in (3, 1, 2):
+        remote(xzs.at[block], xz.at[block], send_z, rz_t, z_device(row_planes[block]))
+
+    send_planes(wgu, zgu, rz_gu, FAR_FIRST)
+    send_planes(wd, zd, rz_d, FAR_FIRST)
+    forward(wgu, zl * INPLANE, fgu, z, rp_gu)
     forward(wd, zl * INPLANE, fd, z, rp_d)
+    fgu[z, me] = wgu[zl * INPLANE + me]
+    fd[z, me] = wd[zl * INPLANE + me]
 
     @pl.loop(0, GROUP_ROWS // 16)
     def _(i):
         rows = pl.ds(i * 16, 16)
-        xz[zl, rows, :] = xzs[zl, rows, :]
+        xz[0, rows, :] = xzs[0, rows, :]
 
     def relay(d, src, dst, rz, rp):
         plane = lax.rem(z + PLANES - d, PLANES)
@@ -165,16 +165,13 @@
 
         dst[plane, me] = src[plane, me]
 
-    for d in FAR_FIRST:
-        relay(d, zgu, fgu, rz_gu, rp_gu)
-
     def placed(i):
         within = i % PAIR_ROWS
-        plane = (within >= 3).astype(jnp.int32) + (within >= 6).astype(jnp.int32) + (within >= 9).astype(jnp.int32)
-        at = plane * GROUP_ROWS + (i // PAIR_ROWS) * CAP + within - plane * CAP
+        block = (within >= 3).astype(jnp.int32) + (within >= 6).astype(jnp.int32) + (within >= 9).astype(jnp.int32)
+        at = block * GROUP_ROWS + (i // PAIR_ROWS) * CAP + within - block * CAP
         return jnp.where(within < GROUPS * CAP, at, -1)
 
-    wait_bytes(xz.at[pl.ds(0, GROUPS - 1)], rz_t)
+    wait_bytes(xz.at[pl.ds(1, GROUPS - 1)], rz_t)
     order = (
         placed(lax.broadcasted_iota(jnp.int32, (EXP_ROWS, SLOTS), 0))
         == lax.broadcasted_iota(jnp.int32, (EXP_ROWS, SLOTS), 1)
@@ -190,6 +187,9 @@
         remote(xp.at[place], xe.at[me], send_p, rp_t, device)
 
     xe[me] = xp[me]
+
+    for d in FAR_FIRST:
+        relay(d, zgu, fgu, rz_gu, rp_gu)
 
     for d in FAR_FIRST[:4]:
         relay(d, zd, fd, rz_d, rp_d)
@@ -243,14 +243,10 @@
         wait_bytes(rr.at[n, pl.ds(0, INPLANE - 1)], rp_r.at[n])
         moved = mm(back, rr[n].reshape(EXP_ROWS, COLS))
         q[n] = moved.astype(BF16).reshape(GROUPS, GROUP_ROWS, COLS)
-        for d in (3, 2, 1):
-            for target, there in ((zl + d, zl + d < GROUPS), (zl - d, zl - d >= 0)):
-
-                @pl.when(there)
-                def _(target=target):
-                    remote(q.at[n, target], t.at[n, zl], send_z, rz_r.at[n], (gr, target * 4 + x, tp))
-
-        t[n, zl] = q[n, zl]
+        for block in (3, 1, 2):
+            remote(q.at[n, block], t.at[n, block], send_z, rz_r.at[n], z_device(row_sources[block]))
+
+        t[n, 0] = q[n, 0]
 
     down_copy = pltpu.make_async_copy(dn, down_out.at[0], out_sem.at[2])
     down_copy.start()
@@ -268,7 +264,7 @@
     weights = [jnp.broadcast_to(weight[k : k + 1, :], (128, TOK)).T[:, 0:1] for k in range(2)]
     for n in range(NCH):
         cols = slice(n * COLS, (n + 1) * COLS)
-        wait_bytes(t.at[n, pl.ds(0, GROUPS - 1)], rz_r.at[n])
+        wait_bytes(t.at[n, pl.ds(1, GROUPS - 1)], rz_r.at[n])
         table = t[n].reshape(SLOTS, COLS)
         mix[:, cols] = (mm(select[0], table) * weights[0] + mm(select[1], table) * weights[1]).astype(BF16)
     mixed_copy = pltpu.make_async_copy(mix, mixed_out, out_sem.at[3])

time: 188 us -> 151 us (0.80)
  Pallas kernels: 181 us -> 144 us
    pallas_call x1, Pallas kernels: 181 us -> 144 us  [body(): pl.pallas_call(kernel, out_shape=(jax.ShapeDtypeStruct((1, D, F), BF16),...]
where the time goes in v2:
time: 151 us
  Pallas kernels  144 us (95%)
  local copies, waits for them, and re-layouts  6.15 us (4%)
    pallas_call x1, Pallas kernels, body(): pl.pallas_call(kernel, out_shape=(jax.ShapeDtypeStruct((1, D, F), BF16),...  144 us
    unnamed x10, local copies, waits for them, and re-layouts  6.15 us

profile of v2, /device:TPU:1, one launch (start us, length us, event | category | flops | bytes accessed | tf_op | source)
XLA Modules:
  0.0 151.2 jit_solution(7556443170347635215)
XLA Ops:
  0.6 144.4 %shard_map.111 = (bf16[1,2048,256]{2,1,0:T(8,128)(2,1)}, bf16[1,2048,256]{2,1,0:T(8,128)(2,1)}, bf16[1,256,2048]{2,1,0:T(8,128)(2,1)}, bf16[128,2048]{1,0:T(8,128)(2,1)}) custom-call(f32[128,16,128]{2,1,0:T(8,128)} %bitcast.6, f32[128,16,128]{2,1,0:T(8,128)} %bitcast.7, f32[128,16,128]{2,1,0:T(8,128)} %down_in.1, f32[1,128]{1,0:T(1,128)} %bitcast.10, ...), custom_call_target="tpu_custom_call" | custom-call | tf_op jit(solution)/shard_map/pallas_call | solution.py:295
  145.0 0.0 copy-start.1
  145.0 2.4 %copy.16 = bf16[1,2048,256]{2,1,0:T(8,128)(2,1)} copy(bf16[1,2048,256]{2,1,0:T(8,128)(2,1)} %get-tuple-element.8) | data formatting | bytes 2097152
  147.4 0.0 copy-done.1
  147.4 0.0 copy-start
  147.4 1.0 copy.17
  148.4 0.6 copy-done
  149.0 0.0 copy-start.2
  149.0 1.0 copy.18
  150.0 0.4 copy-done.2
  150.4 0.8 copy.19
Async XLA Ops:
  145.0 2.4 %copy-start.1 = (bf16[1,2048,256]{2,1,0:T(8,128)(2,1)S(1)}, bf16[1,2048,256]{2,1,0:T(8,128)(2,1)}, u32[]{:S(2)}) copy-start(bf16[1,2048,256]{2,1,0:T(8,128)(2,1)} %get-tuple-element.9) | copy-start | bytes 3145732
  147.4 1.6 %copy-start = (bf16[1,256,2048]{2,1,0:T(8,128)(2,1)S(1)}, bf16[1,256,2048]{2,1,0:T(8,128)(2,1)}, u32[]{:S(2)}) copy-start(bf16[1,256,2048]{2,1,0:T(8,128)(2,1)} %get-tuple-element.10) | copy-start | bytes 3145732
  149.0 1.4 copy-start.2

commit v3 on v2

--- a/solution.py
+++ b/solution.py
@@ -18,6 +18,9 @@
 PAIR_ROWS = 16
 EXP_ROWS = INPLANE * PAIR_ROWS
 NCH = 4
+PIECE = 8
+PIECE_ROWS = INPLANE * PIECE
+PIECES = NCH + NCH // 2
 COLS = D // NCH
 FAR_FIRST = (4, 3, 5, 2, 6, 1, 7)
 
@@ -165,17 +168,19 @@
 
         dst[plane, me] = src[plane, me]
 
-    def placed(i):
-        within = i % PAIR_ROWS
+    def placed(place, within):
         block = (within >= 3).astype(jnp.int32) + (within >= 6).astype(jnp.int32) + (within >= 9).astype(jnp.int32)
-        at = block * GROUP_ROWS + (i // PAIR_ROWS) * CAP + within - block * CAP
+        at = block * GROUP_ROWS + place * CAP + within - block * CAP
         return jnp.where(within < GROUPS * CAP, at, -1)
 
+    def onehot(mask):
+        return mask.astype(F32).astype(BF16)
+
     wait_bytes(xz.at[pl.ds(1, GROUPS - 1)], rz_t)
-    order = (
-        placed(lax.broadcasted_iota(jnp.int32, (EXP_ROWS, SLOTS), 0))
-        == lax.broadcasted_iota(jnp.int32, (EXP_ROWS, SLOTS), 1)
-    ).astype(F32).astype(BF16)
+    to = lax.broadcasted_iota(jnp.int32, (EXP_ROWS, SLOTS), 0)
+    order = onehot(
+        placed(to // PAIR_ROWS, to % PAIR_ROWS) == lax.broadcasted_iota(jnp.int32, (EXP_ROWS, SLOTS), 1)
+    )
     for n in range(NCH):
         cols = slice(n * COLS, (n + 1) * COLS)
         moved = mm(order, xz[:, :, cols].reshape(SLOTS, COLS))
@@ -223,25 +228,40 @@
                     dn[(s * 4 + px) * 16 : (s * 4 + px + 1) * 16, col * 128 : (col + 1) * 128] = fd[
                         h * 4 + s, px * 8 + place
                     ]
-    for n in range(NCH):
-        cols = slice(n * COLS, (n + 1) * COLS)
-        result = mm(hid[...], dn[:, cols])
-        r[n] = result.astype(BF16).reshape(INPLANE, PAIR_ROWS, COLS)
+    piece_row = lax.broadcasted_iota(jnp.int32, (PIECE_ROWS, EXP_ROWS), 0)
+    exp_row = lax.broadcasted_iota(jnp.int32, (PIECE_ROWS, EXP_ROWS), 1)
+    tile_row = piece_row // PIECE * PAIR_ROWS
+    first = mm(onehot(exp_row == tile_row + piece_row % PIECE), hid[...]).astype(BF16)
+    last = mm(onehot(exp_row == tile_row + PIECE + piece_row % 4), hid[...]).astype(BF16)
+    lower = lax.broadcasted_iota(jnp.int32, (PIECE_ROWS, COLS), 0) % PIECE < 4
+
+    def send_piece(k, result):
+        r[k] = result.astype(BF16).reshape(INPLANE, PIECE, COLS)
 
         @pl.loop(1, INPLANE)
         def _(j):
             place, device = hop(j)
-            remote(r.at[n, place], rr.at[n, me], send_p, rp_r.at[n], device)
-
-        rr[n, me] = r[n, me]
-
-    back = (
-        placed(lax.broadcasted_iota(jnp.int32, (SLOTS, EXP_ROWS), 1))
-        == lax.broadcasted_iota(jnp.int32, (SLOTS, EXP_ROWS), 0)
-    ).astype(F32).astype(BF16)
+            remote(r.at[k, place], rr.at[k, me], send_p, rp_r.at[k], device)
+
+        rr[k, me] = r[k, me]
+
+    for m in range(2):
+        even, odd = (dn[:, n * COLS : (n + 1) * COLS] for n in (2 * m, 2 * m + 1))
+        send_piece(2 * m, mm(first, even))
+        send_piece(NCH + m, jnp.where(lower, mm(last, even), mm(last, odd)))
+        send_piece(2 * m + 1, mm(first, odd))
+
+    slot_row = lax.broadcasted_iota(jnp.int32, (SLOTS, PIECE_ROWS), 0)
+    from_row = lax.broadcasted_iota(jnp.int32, (SLOTS, PIECE_ROWS), 1)
+    back = onehot(placed(from_row // PIECE, from_row % PIECE) == slot_row)
+    is_last = placed(from_row // PIECE, PIECE + from_row % 4) == slot_row
+    back_last = [onehot(is_last & (from_row % PIECE // 4 == h)) for h in range(2)]
     for n in range(NCH):
         wait_bytes(rr.at[n, pl.ds(0, INPLANE - 1)], rp_r.at[n])
-        moved = mm(back, rr[n].reshape(EXP_ROWS, COLS))
+        tail = NCH + n // 2
+        if n % 2 == 0:
+            wait_bytes(rr.at[tail, pl.ds(0, INPLANE - 1)], rp_r.at[tail])
+        moved = mm(back, rr[n].reshape(PIECE_ROWS, COLS)) + mm(back_last[n % 2], rr[tail].reshape(PIECE_ROWS, COLS))
         q[n] = moved.astype(BF16).reshape(GROUPS, GROUP_ROWS, COLS)
         for block in (3, 1, 2):
             remote(q.at[n, block], t.at[n, block], send_z, rz_r.at[n], z_device(row_sources[block]))
@@ -279,29 +299,52 @@
     wait_bytes(xe.at[pl.ds(0, INPLANE - 1)], send_p)
     for n in range(NCH):
         wait_bytes(t.at[n, pl.ds(0, GROUPS - 1)], send_z)
-        wait_bytes(rr.at[n, pl.ds(0, INPLANE - 1)], send_p)
+    for k in range(PIECES):
+        wait_bytes(rr.at[k, pl.ds(0, INPLANE - 1)], send_p)
     down_copy.wait()
     gate_copy.wait()
     up_copy.wait()
     mixed_copy.wait()
 
 
+def write_out(*refs):
+    srcs, dsts, bufs, in_sem, out_sem = refs[0:4], refs[4:8], refs[8:12], refs[12], refs[13]
+    pieces = []
+    for i in range(4):
+        rows = srcs[i].shape[-2] // 2
+        for h in range(2):
+            cut = (0,) * (len(srcs[i].shape) - 2) + (pl.ds(h * rows, rows),)
+            n = 2 * i + h
+            pieces.append((
+                pltpu.make_async_copy(srcs[i].at[cut], bufs[i].at[cut], in_sem.at[n]),
+                pltpu.make_async_copy(bufs[i].at[cut], dsts[i].at[cut], out_sem.at[n]),
+            ))
+    for load, _ in pieces:
+        load.start()
+    for load, store in pieces:
+        load.wait()
+        store.start()
+    for _, store in pieces:
+        store.wait()
+
+
 def body(
     tokens, norm_gain, gate_master, up_master, down_master, route_group, route_expert, route_weight
 ):
-    vmem, hbm = pl.BlockSpec(memory_space=pltpu.VMEM), pl.BlockSpec(memory_space=pl.ANY)
+    vmem, hbm = pl.BlockSpec(memory_space=pltpu.VMEM), pl.BlockSpec(memory_space=pltpu.HBM)
     dma = pltpu.SemaphoreType.DMA
     tile = pltpu.VMEM
-    return pl.pallas_call(
+    shapes = (
+        jax.ShapeDtypeStruct((1, D, F), BF16),
+        jax.ShapeDtypeStruct((1, D, F), BF16),
+        jax.ShapeDtypeStruct((1, F, D), BF16),
+        jax.ShapeDtypeStruct((TOK, D), BF16),
+    )
+    outs = pl.pallas_call(
         kernel,
-        out_shape=(
-            jax.ShapeDtypeStruct((1, D, F), BF16),
-            jax.ShapeDtypeStruct((1, D, F), BF16),
-            jax.ShapeDtypeStruct((1, F, D), BF16),
-            jax.ShapeDtypeStruct((TOK, D), BF16),
-        ),
+        out_shape=shapes,
         in_specs=[hbm, hbm, hbm, vmem, hbm, vmem, vmem, vmem],
-        out_specs=(hbm, hbm, hbm, hbm),
+        out_specs=(hbm,) * 4,
         scratch_shapes=[
             tile((3, 128, 16, 128), F32),
             tile((128, 32, 128), BF16),
@@ -321,8 +364,8 @@
             tile((F, D), BF16),
             tile((D, F), BF16),
             tile((D, F), BF16),
-            tile((NCH, INPLANE, PAIR_ROWS, COLS), BF16),
-            tile((NCH, INPLANE, PAIR_ROWS, COLS), BF16),
+            tile((PIECES, INPLANE, PIECE, COLS), BF16),
+            tile((PIECES, INPLANE, PIECE, COLS), BF16),
             tile((NCH, GROUPS, GROUP_ROWS, COLS), BF16),
             tile((NCH, GROUPS, GROUP_ROWS, COLS), BF16),
             tile((TOK, D), BF16),
@@ -337,7 +380,7 @@
             dma,
             dma,
             dma,
-            dma((NCH,)),
+            dma((PIECES,)),
         ],
         compiler_params=pltpu.CompilerParams(
             collective_id=0, has_side_effects=True, vmem_limit_bytes=60 * 2**20
@@ -352,6 +395,14 @@
         route_expert.T,
         route_weight.T,
     )
+    return pl.pallas_call(
+        write_out,
+        out_shape=shapes,
+        in_specs=[hbm] * 4,
+        out_specs=(hbm,) * 4,
+        scratch_shapes=[tile(a.shape, a.dtype) for a in shapes] + [dma((8,)), dma((8,))],
+        compiler_params=pltpu.CompilerParams(vmem_limit_bytes=60 * 2**20),
+    )(*outs)
 
 
 def solution(mesh):

time: 151 us -> 145 us (0.960)
  local copies, waits for them, and re-layouts: 6.15 us -> 0 us
    unnamed x10 -> x0, local copies, waits for them, and re-layouts: 6.15 us -> none
    pallas_call x1 -> x2, Pallas kernels: 144 us -> 144 us  [the longest x1 141 us: body(): pl.pallas_call(kernel, out_shape=shapes, in_specs=[hbm, hbm, hbm, vmem, h...]
where the time goes in v3:
time: 145 us
  Pallas kernels  144 us (99%)
    pallas_call x1, Pallas kernels, body(): pl.pallas_call(kernel, out_shape=shapes, in_specs=[hbm, hbm, hbm, vmem, h...  141 us
    pallas_call x1, Pallas kernels, body(): pl.pallas_call(write_out, out_shape=shapes, in_specs=[hbm] * 4, out_specs...  3.01 us

profile of v3, /device:TPU:1, one launch (start us, length us, event | category | flops | bytes accessed | tf_op | source)
XLA Modules:
  0.0 144.6 jit_solution(3195693612900886143)
XLA Ops:
  0.6 141.0 %shard_map.111 = (bf16[1,2048,256]{2,1,0:T(8,128)(2,1)}, bf16[1,2048,256]{2,1,0:T(8,128)(2,1)}, bf16[1,256,2048]{2,1,0:T(8,128)(2,1)}, bf16[128,2048]{1,0:T(8,128)(2,1)}) custom-call(f32[128,16,128]{2,1,0:T(8,128)} %bitcast.6, f32[128,16,128]{2,1,0:T(8,128)} %bitcast.7, f32[128,16,128]{2,1,0:T(8,128)} %down_in.1, f32[1,128]{1,0:T(1,128)} %bitcast.10, ...), custom_call_target="tpu_custom_call" | custom-call | tf_op jit(solution)/shard_map/pallas_call | solution.py:343
  141.6 3.0 %shard_map.112 = (bf16[1,2048,256]{2,1,0:T(8,128)(2,1)}, bf16[1,2048,256]{2,1,0:T(8,128)(2,1)}, bf16[1,256,2048]{2,1,0:T(8,128)(2,1)}, bf16[128,2048]{1,0:T(8,128)(2,1)}) custom-call(bf16[1,2048,256]{2,1,0:T(8,128)(2,1)} %get-tuple-element.8.refs_0_, bf16[1,2048,256]{2,1,0:T(8,128)(2,1)} %get-tuple-element.9.refs_1_, ...), custom_call_target="tpu_custom_call" | custom-call | tf_op jit(solution)/shard_map/pallas_call | solution.py:398

commit v4 on v3

--- a/solution.py
+++ b/solution.py
@@ -22,7 +22,7 @@
 PIECE_ROWS = INPLANE * PIECE
 PIECES = NCH + NCH // 2
 COLS = D // NCH
-FAR_FIRST = (4, 3, 5, 2, 6, 1, 7)
+NEAR_FIRST = (1, 7, 2, 6, 3, 5, 4)
 
 
 def nt_dot(a, b):
@@ -54,7 +54,7 @@
         return (lax.div(target, 4), lax.rem(target, 4) * 4 + x, tp)
 
     def hop(j):
-        o = lax.rem(j * 11, INPLANE)
+        o = lax.rem(j * 21, INPLANE)
         tx = lax.rem(x + lax.div(o, 8), 4)
         ty = lax.rem(y + lax.rem(lax.div(o, 2), 4), 4)
         ttp = ty * 2 + lax.rem(c + lax.rem(o, 2), 2)
@@ -69,7 +69,7 @@
         pltpu.make_async_copy(ref, ref, sem).wait()
 
     barrier = pltpu.get_barrier_semaphore()
-    for d in FAR_FIRST:
+    for d in NEAR_FIRST:
         pl.semaphore_signal(barrier, inc=1, device_id=z_device(lax.rem(z + d, PLANES)), device_id_type=MESH)
 
     @pl.loop(1, INPLANE)
@@ -128,7 +128,7 @@
         e = pl.ds(i * 8, 8)
         wd[e] = fbuf[2, e].astype(BF16)
 
-    pl.semaphore_wait(barrier, len(FAR_FIRST) + INPLANE - 1)
+    pl.semaphore_wait(barrier, len(NEAR_FIRST) + INPLANE - 1)
 
     def send_planes(src, dst, recv, steps):
         for d in steps:
@@ -145,8 +145,8 @@
     for block in (3, 1, 2):
         remote(xzs.at[block], xz.at[block], send_z, rz_t, z_device(row_planes[block]))
 
-    send_planes(wgu, zgu, rz_gu, FAR_FIRST)
-    send_planes(wd, zd, rz_d, FAR_FIRST)
+    send_planes(wgu, zgu, rz_gu, NEAR_FIRST)
+    send_planes(wd, zd, rz_d, NEAR_FIRST)
     forward(wgu, zl * INPLANE, fgu, z, rp_gu)
     forward(wd, zl * INPLANE, fd, z, rp_d)
     fgu[z, me] = wgu[zl * INPLANE + me]
@@ -193,10 +193,10 @@
 
     xe[me] = xp[me]
 
-    for d in FAR_FIRST:
+    for d in NEAR_FIRST:
         relay(d, zgu, fgu, rz_gu, rp_gu)
 
-    for d in FAR_FIRST[:4]:
+    for d in NEAR_FIRST[:4]:
         relay(d, zd, fd, rz_d, rp_d)
 
     wait_bytes(fgu.at[:, pl.ds(0, INPLANE - 1)], rp_gu)
@@ -216,7 +216,7 @@
         upper = nt_dot(rows, ut[...])
         hid[pl.ds(i * 128, 128), :] = (gate / (1.0 + jnp.exp(-gate)) * upper).astype(BF16)
 
-    for d in FAR_FIRST[4:]:
+    for d in NEAR_FIRST[4:]:
         relay(d, zd, fd, rz_d, rp_d)
 
     wait_bytes(fd.at[:, pl.ds(0, INPLANE - 1)], rp_d)

time: 145 us -> 141 us (0.972)
  Pallas kernels: 144 us -> 140 us
    pallas_call x1, Pallas kernels: 141 us -> 137 us  [body(): pl.pallas_call(kernel, out_shape=shapes, in_specs=[hbm, hbm, hbm, vmem, h...]
where the time goes in v4:
time: 141 us
  Pallas kernels  140 us (99%)
    pallas_call x1, Pallas kernels, body(): pl.pallas_call(kernel, out_shape=shapes, in_specs=[hbm, hbm, hbm, vmem, h...  137 us
    pallas_call x1, Pallas kernels, body(): pl.pallas_call(write_out, out_shape=shapes, in_specs=[hbm] * 4, out_specs...  3.01 us

profile of v4, /device:TPU:1, one launch (start us, length us, event | category | flops | bytes accessed | tf_op | source)
XLA Modules:
  0.0 140.7 jit_solution(10033870947484361065)
XLA Ops:
  0.6 137.0 %shard_map.111 = (bf16[1,2048,256]{2,1,0:T(8,128)(2,1)}, bf16[1,2048,256]{2,1,0:T(8,128)(2,1)}, bf16[1,256,2048]{2,1,0:T(8,128)(2,1)}, bf16[128,2048]{1,0:T(8,128)(2,1)}) custom-call(f32[128,16,128]{2,1,0:T(8,128)} %bitcast.6, f32[128,16,128]{2,1,0:T(8,128)} %bitcast.7, f32[128,16,128]{2,1,0:T(8,128)} %down_in.1, f32[1,128]{1,0:T(1,128)} %bitcast.10, ...), custom_call_target="tpu_custom_call" | custom-call | tf_op jit(solution)/shard_map/pallas_call | solution.py:343
  137.7 3.0 %shard_map.112 = (bf16[1,2048,256]{2,1,0:T(8,128)(2,1)}, bf16[1,2048,256]{2,1,0:T(8,128)(2,1)}, bf16[1,256,2048]{2,1,0:T(8,128)(2,1)}, bf16[128,2048]{1,0:T(8,128)(2,1)}) custom-call(bf16[1,2048,256]{2,1,0:T(8,128)(2,1)} %get-tuple-element.8.refs_0_, bf16[1,2048,256]{2,1,0:T(8,128)(2,1)} %get-tuple-element.9.refs_1_, ...), custom_call_target="tpu_custom_call" | custom-call | tf_op jit(solution)/shard_map/pallas_call | solution.py:398

commit v5 on v4

--- a/solution.py
+++ b/solution.py
@@ -15,8 +15,6 @@
 TOK, D, F, CAP = 128, 2048, 256, 3
 GROUP_ROWS = INPLANE * CAP
 SLOTS = GROUPS * GROUP_ROWS
-PAIR_ROWS = 16
-EXP_ROWS = INPLANE * PAIR_ROWS
 NCH = 4
 PIECE = 8
 PIECE_ROWS = INPLANE * PIECE
@@ -37,7 +35,7 @@
     gate_in, up_in, down_in, gain, tok_in, group, expert, weight,
     gate_out, up_out, down_out, mixed_out,
     fbuf, wgu, wd, zgu, zd, fgu, fd,
-    tokv, xzs, xz, xp, xe, hid,
+    tokv, xzs, xz, xp, xpl, xe, xel, xl, hid, hidl,
     gt, ut, dn, go, uo, r, rr, q, t, mix,
     in_sem, out_sem, send_z, send_p, rz_gu, rz_d, rz_t, rz_r, rp_gu, rp_d, rp_t, rp_r,
 ):
@@ -177,21 +175,29 @@
         return mask.astype(F32).astype(BF16)
 
     wait_bytes(xz.at[pl.ds(1, GROUPS - 1)], rz_t)
-    to = lax.broadcasted_iota(jnp.int32, (EXP_ROWS, SLOTS), 0)
-    order = onehot(
-        placed(to // PAIR_ROWS, to % PAIR_ROWS) == lax.broadcasted_iota(jnp.int32, (EXP_ROWS, SLOTS), 1)
-    )
+    to = lax.broadcasted_iota(jnp.int32, (PIECE_ROWS, SLOTS), 0)
+    of = lax.broadcasted_iota(jnp.int32, (PIECE_ROWS, SLOTS), 1)
+    order = onehot(placed(to // PIECE, to % PIECE) == of)
+    order_last = onehot(placed(to // PIECE, PIECE + to % 4) == of)
+    lower = lax.broadcasted_iota(jnp.int32, (PIECE_ROWS, COLS), 0) % PIECE < 4
+    halves = []
     for n in range(NCH):
         cols = slice(n * COLS, (n + 1) * COLS)
-        moved = mm(order, xz[:, :, cols].reshape(SLOTS, COLS))
-        xp[:, :, cols] = moved.astype(BF16).reshape(INPLANE, PAIR_ROWS, COLS)
+        rows = xz[:, :, cols].reshape(SLOTS, COLS)
+        xp[:, :, cols] = mm(order, rows).astype(BF16).reshape(INPLANE, PIECE, COLS)
+        halves.append(mm(order_last, rows))
+    for m in range(NCH // 2):
+        both = jnp.where(lower, halves[m], halves[m + NCH // 2])
+        xpl[:, :, m * COLS : (m + 1) * COLS] = both.astype(BF16).reshape(INPLANE, PIECE, COLS)
 
     @pl.loop(1, INPLANE)
     def _(j):
         place, device = hop(j)
-        remote(xp.at[place], xe.at[me], send_p, rp_t, device)
+        remote(xp.at[place], xe.at[me], send_p, rp_t.at[0], device)
+        remote(xpl.at[place], xel.at[me], send_p, rp_t.at[1], device)
 
     xe[me] = xp[me]
+    xel[me] = xpl[me]
 
     for d in NEAR_FIRST:
         relay(d, zgu, fgu, rz_gu, rp_gu)
@@ -207,14 +213,27 @@
                 tiles = slice(px * 8, (px + 1) * 8)
                 gt[rows, cols] = fgu[h * 4 + s, tiles, 0:16, :].reshape(128, 128)
                 ut[rows, cols] = fgu[h * 4 + s, tiles, 16:32, :].reshape(128, 128)
-    wait_bytes(xe.at[pl.ds(0, INPLANE - 1)], rp_t)
-
-    @pl.loop(0, EXP_ROWS // 128)
-    def _(i):
-        rows = xe[pl.ds(i * 8, 8)].reshape(128, D)
+    wait_bytes(xe.at[pl.ds(0, INPLANE - 1)], rp_t.at[0])
+    wait_bytes(xel.at[pl.ds(0, INPLANE - 1)], rp_t.at[1])
+
+    def hidden(rows):
         gate = nt_dot(rows, gt[...])
         upper = nt_dot(rows, ut[...])
-        hid[pl.ds(i * 128, 128), :] = (gate / (1.0 + jnp.exp(-gate)) * upper).astype(BF16)
+        return (gate / (1.0 + jnp.exp(-gate)) * upper).astype(BF16)
+
+    @pl.loop(0, PIECE_ROWS // 128)
+    def _(i):
+        hid[pl.ds(i * 128, 128), :] = hidden(xe[pl.ds(i * 16, 16)].reshape(128, D))
+
+    last_row = lax.broadcasted_iota(jnp.int32, (128, PIECE_ROWS), 0)
+    tail_row = lax.broadcasted_iota(jnp.int32, (128, PIECE_ROWS), 1)
+    for h in range(2):
+        unstack = onehot(tail_row == last_row // 4 * PIECE + h * 4 + last_row % 4)
+        for m in range(NCH // 2):
+            at = h * (D // 2) + m * COLS
+            tail = xel[:, :, m * COLS : (m + 1) * COLS].reshape(PIECE_ROWS, COLS)
+            xl[:, at : at + COLS] = mm(unstack, tail).astype(BF16)
+    hidl[...] = hidden(xl[...])
 
     for d in NEAR_FIRST[4:]:
         relay(d, zd, fd, rz_d, rp_d)
@@ -228,12 +247,10 @@
                     dn[(s * 4 + px) * 16 : (s * 4 + px + 1) * 16, col * 128 : (col + 1) * 128] = fd[
                         h * 4 + s, px * 8 + place
                     ]
-    piece_row = lax.broadcasted_iota(jnp.int32, (PIECE_ROWS, EXP_ROWS), 0)
-    exp_row = lax.broadcasted_iota(jnp.int32, (PIECE_ROWS, EXP_ROWS), 1)
-    tile_row = piece_row // PIECE * PAIR_ROWS
-    first = mm(onehot(exp_row == tile_row + piece_row % PIECE), hid[...]).astype(BF16)
-    last = mm(onehot(exp_row == tile_row + PIECE + piece_row % 4), hid[...]).astype(BF16)
-    lower = lax.broadcasted_iota(jnp.int32, (PIECE_ROWS, COLS), 0) % PIECE < 4
+    piece_row = lax.broadcasted_iota(jnp.int32, (PIECE_ROWS, 128), 0)
+    last_of = lax.broadcasted_iota(jnp.int32, (PIECE_ROWS, 128), 1)
+    first = hid[...]
+    last = mm(onehot(last_of == piece_row // PIECE * 4 + piece_row % 4), hidl[...]).astype(BF16)
 
     def send_piece(k, result):
         r[k] = result.astype(BF16).reshape(INPLANE, PIECE, COLS)
@@ -297,6 +314,7 @@
     wait_bytes(fgu.at[:, pl.ds(0, INPLANE - 1)], send_p)
     wait_bytes(fd.at[:, pl.ds(0, INPLANE - 1)], send_p)
     wait_bytes(xe.at[pl.ds(0, INPLANE - 1)], send_p)
+    wait_bytes(xel.at[pl.ds(0, INPLANE - 1)], send_p)
     for n in range(NCH):
         wait_bytes(t.at[n, pl.ds(0, GROUPS - 1)], send_z)
     for k in range(PIECES):
@@ -356,9 +374,13 @@
             tile((TOK, D), BF16),
             tile((GROUPS, GROUP_ROWS, D), BF16),
             tile((GROUPS, GROUP_ROWS, D), BF16),
-            tile((INPLANE, PAIR_ROWS, D), BF16),
-            tile((INPLANE, PAIR_ROWS, D), BF16),
-            tile((EXP_ROWS, F), BF16),
+            tile((INPLANE, PIECE, D), BF16),
+            tile((INPLANE, PIECE, D // 2), BF16),
+            tile((INPLANE, PIECE, D), BF16),
+            tile((INPLANE, PIECE, D // 2), BF16),
+            tile((128, D), BF16),
+            tile((PIECE_ROWS, F), BF16),
+            tile((128, F), BF16),
             tile((F, D), BF16),
             tile((F, D), BF16),
             tile((F, D), BF16),
@@ -379,7 +401,7 @@
             dma((NCH,)),
             dma,
             dma,
-            dma,
+            dma((2,)),
             dma((PIECES,)),
         ],
         compiler_params=pltpu.CompilerParams(

time: 141 us -> 140 us (level)
  no operation moved by 1% of the time
where the time goes in v5:
time: 140 us
  Pallas kernels  140 us (100%)
    pallas_call x1, Pallas kernels, body(): pl.pallas_call(kernel, out_shape=shapes, in_specs=[hbm, hbm, hbm, vmem, h...  137 us
    pallas_call x1, Pallas kernels, body(): pl.pallas_call(write_out, out_shape=shapes, in_specs=[hbm] * 4, out_specs...  3.01 us

profile of v5, /device:TPU:1, one launch (start us, length us, event | category | flops | bytes accessed | tf_op | source)
XLA Modules:
  0.0 140.2 jit_solution(18139128591894652806)
XLA Ops:
  0.6 136.6 %shard_map.111 = (bf16[1,2048,256]{2,1,0:T(8,128)(2,1)}, bf16[1,2048,256]{2,1,0:T(8,128)(2,1)}, bf16[1,256,2048]{2,1,0:T(8,128)(2,1)}, bf16[128,2048]{1,0:T(8,128)(2,1)}) custom-call(f32[128,16,128]{2,1,0:T(8,128)} %bitcast.6, f32[128,16,128]{2,1,0:T(8,128)} %bitcast.7, f32[128,16,128]{2,1,0:T(8,128)} %down_in.1, f32[1,128]{1,0:T(1,128)} %bitcast.10, ...), custom_call_target="tpu_custom_call" | custom-call | tf_op jit(solution)/shard_map/pallas_call | solution.py:361
  137.2 3.0 %shard_map.112 = (bf16[1,2048,256]{2,1,0:T(8,128)(2,1)}, bf16[1,2048,256]{2,1,0:T(8,128)(2,1)}, bf16[1,256,2048]{2,1,0:T(8,128)(2,1)}, bf16[128,2048]{1,0:T(8,128)(2,1)}) custom-call(bf16[1,2048,256]{2,1,0:T(8,128)(2,1)} %get-tuple-element.8.refs_0_, bf16[1,2048,256]{2,1,0:T(8,128)(2,1)} %get-tuple-element.9.refs_1_, ...), custom_call_target="tpu_custom_call" | custom-call | tf_op jit(solution)/shard_map/pallas_call | solution.py:420

commit v6 on v5

--- a/solution.py
+++ b/solution.py
@@ -329,10 +329,10 @@
     srcs, dsts, bufs, in_sem, out_sem = refs[0:4], refs[4:8], refs[8:12], refs[12], refs[13]
     pieces = []
     for i in range(4):
-        rows = srcs[i].shape[-2] // 2
-        for h in range(2):
+        rows = srcs[i].shape[-2] // 4
+        for h in range(4):
             cut = (0,) * (len(srcs[i].shape) - 2) + (pl.ds(h * rows, rows),)
-            n = 2 * i + h
+            n = 4 * i + h
             pieces.append((
                 pltpu.make_async_copy(srcs[i].at[cut], bufs[i].at[cut], in_sem.at[n]),
                 pltpu.make_async_copy(bufs[i].at[cut], dsts[i].at[cut], out_sem.at[n]),
@@ -422,7 +422,7 @@
         out_shape=shapes,
         in_specs=[hbm] * 4,
         out_specs=(hbm,) * 4,
-        scratch_shapes=[tile(a.shape, a.dtype) for a in shapes] + [dma((8,)), dma((8,))],
+        scratch_shapes=[tile(a.shape, a.dtype) for a in shapes] + [dma((16,)), dma((16,))],
         compiler_params=pltpu.CompilerParams(vmem_limit_bytes=60 * 2**20),
     )(*outs)
 

time: 140 us -> 141 us (level)
  no operation moved by 1% of the time
where the time goes in v6:
time: 141 us; the launch traced here: 140 us
  Pallas kernels  140 us (99%)
    pallas_call x1, Pallas kernels, body(): pl.pallas_call(kernel, out_shape=shapes, in_specs=[hbm, hbm, hbm, vmem, h...  137 us
    pallas_call x1, Pallas kernels, body(): pl.pallas_call(write_out, out_shape=shapes, in_specs=[hbm] * 4, out_specs...  3.24 us

profile of v6, /device:TPU:1, one launch (start us, length us, event | category | flops | bytes accessed | tf_op | source)
XLA Modules:
  0.0 140.4 jit_solution(1373541181660874171)
XLA Ops:
  0.6 136.6 %shard_map.111 = (bf16[1,2048,256]{2,1,0:T(8,128)(2,1)}, bf16[1,2048,256]{2,1,0:T(8,128)(2,1)}, bf16[1,256,2048]{2,1,0:T(8,128)(2,1)}, bf16[128,2048]{1,0:T(8,128)(2,1)}) custom-call(f32[128,16,128]{2,1,0:T(8,128)} %bitcast.6, f32[128,16,128]{2,1,0:T(8,128)} %bitcast.7, f32[128,16,128]{2,1,0:T(8,128)} %down_in.1, f32[1,128]{1,0:T(1,128)} %bitcast.10, ...), custom_call_target="tpu_custom_call" | custom-call | tf_op jit(solution)/shard_map/pallas_call | solution.py:361
  137.2 3.2 %shard_map.112 = (bf16[1,2048,256]{2,1,0:T(8,128)(2,1)}, bf16[1,2048,256]{2,1,0:T(8,128)(2,1)}, bf16[1,256,2048]{2,1,0:T(8,128)(2,1)}, bf16[128,2048]{1,0:T(8,128)(2,1)}) custom-call(bf16[1,2048,256]{2,1,0:T(8,128)(2,1)} %get-tuple-element.8.refs_0_, bf16[1,2048,256]{2,1,0:T(8,128)(2,1)} %get-tuple-element.9.refs_1_, ...), custom_call_target="tpu_custom_call" | custom-call | tf_op jit(solution)/shard_map/pallas_call | solution.py:420
